TPU v7x, 128 devices: a whole 4x4x4 slice. The times are simulated.
128 devices in a mesh: sp: 16 (over z, x), tp: 8 (over y, core).
Axes of the slice: x: 4, y: 4, z: 4, core: 2. Of those that a mesh axis runs over, the one named last changes fastest.
Arguments:
- query_small: bfloat16 [12288, 1024], P('sp', 'tp'), may hold values from -18 to 18
- key_small: bfloat16 [12288, 1024], P('sp', 'tp'), may hold values from -6 to 6
- value_small: bfloat16 [12288, 1024], P('sp', 'tp'), may hold values from -6 to 6
- offset_small: bfloat16 [16, 12288], P('tp', 'sp'), may hold values from -25 to 0
- query_large: bfloat16 [12288, 1024], P('sp', 'tp'), may hold values from -18 to 18
- key_large: bfloat16 [12288, 1024], P('sp', 'tp'), may hold values from -6 to 6
- value_large: bfloat16 [12288, 1024], P('sp', 'tp'), may hold values from -6 to 6
- offset_large: bfloat16 [8, 12288], P('tp', 'sp'), may hold values from -25 to 0
- out_small: bfloat16 [1024, 2048], P('tp'), may hold values from -0.125 to 0.125
- out_large: bfloat16 [1024, 2048], P('tp'), may hold values from -0.125 to 0.125
- residual: bfloat16 [12288, 2048], P(('sp', 'tp')), may hold values from -1.1953125 to 1.1953125
- norm_gain: bfloat16 [2048], replicated, may hold values from 0.099609375 to 1.8984375
- gate_weight: bfloat16 [2048, 5632], P('sp', 'tp'), may hold values from -0.125 to 0.125
- up_weight: bfloat16 [2048, 5632], P('sp', 'tp'), may hold values from -0.125 to 0.125
- down_weight: bfloat16 [5632, 2048], P('tp', 'sp'), may hold values from -0.078125 to 0.078125
Outputs:
- layer_out: bfloat16 [12288, 2048], P(('sp', 'tp'))
All inputs are finite; a program needn't handle non-finite values.
Results may differ from a plain program's by a relative error of at most 0.023.
Values may be sent and summed in bfloat16 or wider, within the bound.
No kernel may reach another device: no remote copies, remote signals or barrier semaphores. Data moves between devices by JAX's collectives and lax.ppermute only.
A program may use at most 128 MiB of HBM per device.

v0:
```python
import jax
import jax.numpy as jnp
from jax import lax
from jax.sharding import PartitionSpec as P

SMALL_DIM = 64
LARGE_DIM = 128


def turned_gather(arrays, axis, dims):
    turned = [jnp.moveaxis(a, dim, 0) for a, dim in zip(arrays, dims)]
    both = jnp.concatenate([t.reshape(len(t), -1) for t in turned], axis=1)
    whole, at, done = (lax.all_gather(both, axis, axis=0, tiled=True), 0, [])
    for t, dim in zip(turned, dims):
        share = whole[:, at : at + t[0].size].reshape(-1, *t.shape[1:])
        done.append(jnp.moveaxis(share, 0, dim))
        at += t[0].size
    return tuple(done)


def cut_along(value, dim, length):
    before, after = (value.shape[:dim], value.shape[dim + 1 :])
    return jnp.moveaxis(value.reshape(*before, length, -1, *after), dim, 0)


def summed_on_arrival(value, axis, dim):
    pieces = cut_along(value, dim, lax.axis_size(axis))
    arrived = lax.all_to_all(pieces, axis, split_axis=0, concat_axis=0, tiled=True)
    return arrived.astype(jnp.float32).sum(axis=0)


def split_heads(flat, head_depth):
    return flat.reshape(flat.shape[0], -1, head_depth)


def stick_terms(query, random_keys, values, offset, limits, carried):
    head_depth = query.shape[-1]
    key_heads = split_heads(random_keys, head_depth)
    value_heads = split_heads(values, head_depth)
    logits = jnp.einsum(
        "thd,shd->hts", query, key_heads, preferred_element_type=jnp.float32
    ) * head_depth ** (-0.5)
    logits = logits + offset.astype(jnp.float32)[:, None, :]
    fail_all = jax.nn.log_sigmoid(-logits)
    log_pass = logits + fail_all
    log_fail = fail_all
    before = None
    if limits is not None:
        query_first, key_first = limits
        query_pos = lax.broadcasted_iota(jnp.int32, logits.shape, 1) + query_first
        key_pos = lax.broadcasted_iota(jnp.int32, logits.shape, 2) + key_first
        before = key_pos < query_pos
        log_fail = jnp.where(before, fail_all, 0.0)
    suffix = lax.cumsum(log_fail, axis=2, reverse=True) - log_fail
    weights = jnp.exp(log_pass + suffix + carried[:, :, None])
    if before is not None:
        weights = jnp.where(before, weights, 0.0)
    weights = weights.astype(jnp.bfloat16)
    result = jnp.einsum("hts,shd->thd", weights, value_heads, preferred_element_type=jnp.float32)
    return (result, carried + jnp.sum(log_fail, axis=2))


def both_groups(queries, key_block, limits, totals):
    key_small, value_small, offset_small, key_large, value_large, offset_large = key_block
    out_small, acc_small, out_large, acc_large = totals
    term_small, next_small = stick_terms(
        queries[0], key_small, value_small, offset_small, limits, acc_small
    )
    term_large, next_large = stick_terms(
        queries[1], key_large, value_large, offset_large, limits, acc_large
    )
    return (out_small + term_small, next_small, out_large + term_large, next_large)


def empty_totals(rows, small_heads, large_heads):
    return (
        jnp.zeros((rows, small_heads, SMALL_DIM), jnp.float32),
        jnp.zeros((small_heads, rows), jnp.float32),
        jnp.zeros((rows, large_heads, LARGE_DIM), jnp.float32),
        jnp.zeros((large_heads, rows), jnp.float32),
    )


def rounded(value):
    return lax.optimization_barrier(value.astype(jnp.bfloat16)).astype(jnp.float32)


def rms_norm(stream, gain):
    scale = lax.rsqrt(jnp.mean(stream * stream, axis=-1, keepdims=True) + 1e-06)
    return (stream * scale * gain.astype(jnp.float32)).astype(jnp.bfloat16)


def on_device(
    query_small,
    key_small,
    value_small,
    offset_small,
    query_large,
    key_large,
    value_large,
    offset_large,
    out_small,
    out_large,
    residual,
    norm_gain,
    gate_weight,
    up_weight,
    down_weight,
):
    gate_full, up_full, down_full = turned_gather(
        (gate_weight, up_weight, down_weight), "sp", (0, 0, 1)
    )
    tokens = query_small.shape[0]
    small_heads = offset_small.shape[0]
    large_heads = offset_large.shape[0]
    queries = (split_heads(query_small, SMALL_DIM), split_heads(query_large, LARGE_DIM))
    own_block = (key_small, value_small, offset_small, key_large, value_large, offset_large)
    sp_index = lax.axis_index("sp")
    own_start = sp_index * tokens
    totals = both_groups(
        queries, own_block, (own_start, own_start), empty_totals(tokens, small_heads, large_heads)
    )
    key_dims = (0, 0, 1, 0, 0, 1)
    gathered = turned_gather(
        (own_block[0], own_block[1], own_block[2], own_block[3], own_block[4], own_block[5]),
        "sp",
        (0, 0, 1, 0, 0, 1),
    )

    def far_turn(turn_index, status):
        first_row = (sp_index - 1 - turn_index) * tokens
        key_block = tuple(
            (
                lax.dynamic_slice_in_dim(member, first_row, tokens, member_dim)
                for member, member_dim in zip(gathered, key_dims)
            )
        )
        return both_groups(queries, key_block, None, status)

    totals = lax.fori_loop(0, sp_index, far_turn, totals)
    mixed_small = totals[0].reshape(tokens, -1).astype(jnp.bfloat16)
    mixed_large = totals[2].reshape(tokens, -1).astype(jnp.bfloat16)
    attended = summed_on_arrival(
        (
            jnp.dot(mixed_small, out_small, preferred_element_type=jnp.float32)
            + jnp.dot(mixed_large, out_large, preferred_element_type=jnp.float32)
        ).astype(jnp.bfloat16),
        "tp",
        0,
    )
    stream = residual.astype(jnp.float32) + rounded(attended)
    normed = rms_norm(stream, norm_gain)
    normed_rows = lax.all_gather(normed, "tp", axis=0, tiled=True)
    gate = jnp.dot(normed_rows, gate_full, preferred_element_type=jnp.float32)
    upper = jnp.dot(normed_rows, up_full, preferred_element_type=jnp.float32)
    hidden = (jax.nn.silu(gate) * upper).astype(jnp.bfloat16)
    summed = lax.psum_scatter(
        jnp.dot(hidden, down_full, preferred_element_type=jnp.float32).astype(jnp.bfloat16),
        "tp",
        scatter_dimension=0,
        tiled=True,
    ).astype(jnp.float32)
    return (stream + rounded(summed)).astype(jnp.bfloat16)


def solution(mesh):
    return jax.shard_map(
        on_device,
        mesh=mesh,
        in_specs=(
            P("sp", "tp"),
            P("sp", "tp"),
            P("sp", "tp"),
            P("tp", "sp"),
            P("sp", "tp"),
            P("sp", "tp"),
            P("sp", "tp"),
            P("tp", "sp"),
            P("tp", None),
            P("tp", None),
            P(("sp", "tp"), None),
            P(),
            P("sp", "tp"),
            P("sp", "tp"),
            P("tp", "sp"),
        ),
        out_specs=P(("sp", "tp"), None),
        check_vma=False,
    )
```

profile of v0, /device:TPU:0, one launch (start us, length us, event | category | flops | bytes accessed | tf_op | source)
XLA Modules:
  0.0 1112.9 jit_solution(5923392795557188407)
XLA Ops:
  8.5 3.2 concatenate.6
  13.7 3.2 fusion.59
  17.0 7.7 fusion.38
  27.8 2.4 fusion.54
  30.2 3.9 fusion.60
  34.2 15.1 %fusion.33 = f32[2,768,6,128]{1,2,3,0:T(8,128)S(1)} fusion(f32[2,768,6,128]{1,3,2,0:T(8,128)S(1)} %bitcast.216), kind=kOutput, calls=%fused_computation.58 | output fusion | flops 149815296 | bytes 9437184 | tf_op jit(solution)/shard_map/reduce-window.4
  49.3 2.7 copy-done.4
  52.1 4.7 broadcast_add_fusion.1
  59.3 5.2 fusion.35
  64.6 5.4 fusion.45
  72.4 47.9 %all-gather.4.cloned.1.call-done = bf16[12288,515]{1,0:T(8,128)(2,1)} async-done(((bf16[768,515]{1,0:T(8,128)(2,1)}), bf16[12288,515]{1,0:T(8,128)(2,1)}) %all-gather.4.cloned.1.call-update) | async-done | bytes 12656656 | tf_op jit(solution)/shard_map/all_gather | solution.py:13
  120.3 3.2 slice_bitcast_fusion.3
  123.5 3.2 copy.52
  126.8 3.5 slice_reduce_fusion
  130.3 12.6 %fusion.61 = (bf16[12288,128]{1,0:T(8,128)(2,1)}, bf16[12288,128]{1,0:T(8,128)(2,1)}, bf16[12288,128]{1,0:T(8,128)(2,1)}, bf16[12288,128]{1,0:T(8,128)(2,1)}) fusion(bf16[12288,515]{1,0:T(8,128)(2,1)} %all-gather.4.cloned.1.call-done), kind=kLoop, calls=%fused_computation.112 | loop fusion | bytes 25165824 | tf_op jit(solution)/shard_map/slice | solution.py:15
  145.3 2.7 add_convert_fusion
  148.0 4.6 all-to-all-start
  152.7 38.3 %all-to-all-done = bf16[8,96,2048]{2,1,0:T(8,128)(2,1)} async-done(((bf16[8,96,2048]{2,1,0:T(8,128)(2,1)}), bf16[8,96,2048]{2,1,0:T(8,128)(2,1)}, u32[]{:S(2)}, u32[]{:S(2)}) %all-to-all-start) | async-done | bytes 3145760 | tf_op jit(solution)/shard_map/all_to_all | solution.py:28
  191.0 2.6 reduce_sum.64
  194.8 5.8 all-gather.8.cloned.1.call-done
  200.7 850.6 %all-gather.6.cloned.1.call-done = bf16[768,2048]{1,0:T(8,128)(2,1)} async-done(((bf16[96,2048]{1,0:T(8,128)(2,1)}), bf16[768,2048]{1,0:T(8,128)(2,1)}) %all-gather.6.cloned.1.call-update) | async-done | bytes 3145744 | tf_op jit(solution)/shard_map/all_gather | solution.py:153
  1051.3 5.2 fusion.43
  1056.5 11.8 %convolution_convert_fusion = bf16[768,2048]{1,0:T(8,128)(2,1)} fusion(bf16[2048,2112]{0,1:T(8,128)(2,1)} %all-gather.8.cloned.1.call-done, f32[768,704]{0,1:T(8,128)S(1)} %fusion.43, bf16[768,2048]{1,0:T(8,128)(2,1)} %all-gather.6.cloned.1.call-done), kind=kOutput, calls=%fused_computation.71 | convolution fusion | flops 4434001920 | bytes 14221312 | tf_op jit(solution)/shard_map/dot_general | solution.py:158
  1068.3 36.0 %reduce-scatter.2.cloned.1.call-done = bf16[96,2048]{1,0:T(8,128)(2,1)} async-done(((bf16[768,2048]{1,0:T(8,128)(2,1)}), bf16[96,2048]{1,0:T(8,128)(2,1)}) %reduce-scatter.2.cloned.1.call-update) | async-done | bytes 393232 | tf_op jit(solution)/shard_map/reduce_scatter | solution.py:157
  (89 shorter events, 17.4 us)
Async XLA Ops:
  6.5 137.6 %copy-start = (bf16[128,2048]{1,0:T(8,128)(2,1)S(1)}, bf16[128,2048]{1,0:T(8,128)(2,1)}, u32[]{:S(2)}) copy-start(bf16[128,2048]{1,0:T(8,128)(2,1)} %param.25) | copy-start | bytes 1572868
  6.5 6.1 copy-start.24
  6.5 7.1 copy-start.23
  6.5 6.1 copy-start.14
  6.5 6.3 copy-start.15
  6.6 7.2 copy-start.18
  6.6 5.2 copy-start.20
  6.6 5.2 copy-start.22
  6.6 5.2 copy-start.21
  6.6 7.1 copy-start.26
  6.6 113.7 %all-gather.4.cloned.1.call-start = ((), (), s32[]{:S(2)}) async-start(), calls=%async_computation.2 | async-start | bytes 16711680 | tf_op jit(solution)/shard_map/all_gather | solution.py:13
  11.7 189.0 %all-gather.8.cloned.1.call-start = ((), (), s32[]{:S(2)}) async-start(), calls=%async_computation.4 | async-start | bytes 9191424 | tf_op jit(solution)/shard_map/all_gather | solution.py:13
  17.0 10.0 copy-start.9
  30.1 4.0 copy-start.8
  34.1 15.2 %copy-start.2 = (f32[2,768,768]{1,2,0:T(8,128)}, f32[2,768,768]{1,2,0:T(8,128)S(1)}, u32[]{:S(2)}) copy-start(f32[2,768,768]{1,2,0:T(8,128)S(1)} %get-tuple-element.239) | copy-start | bytes 14155780
  34.1 24.1 %slice-start.2 = ((s8[4718592]{0:T(1024)(128)(4,1)}), s8[524288]{0:T(1024)(128)(4,1)S(1)}, s32[]{:S(2)}) async-start(s8[4718592]{0:T(1024)(128)(4,1)} %bitcast.218), calls=%async_computation.8 | async-start | bytes 1048576
  52.1 6.1 slice-start.3
  64.6 5.4 copy-start.13
  64.6 6.5 copy-start.16
  148.0 4.6 copy-start.25
  148.0 43.0 %all-to-all-start = ((bf16[8,96,2048]{2,1,0:T(8,128)(2,1)}), bf16[8,96,2048]{2,1,0:T(8,128)(2,1)}, u32[]{:S(2)}, u32[]{:S(2)}) async-start(bf16[8,96,2048]{2,1,0:T(8,128)(2,1)} %bitcast.220), calls=%async_computation | async-start | bytes 6291456 | tf_op jit(solution)/shard_map/all_to_all | solution.py:28
  152.6 41.0 %copy-start.10 = (bf16[96,2048]{1,0:T(8,128)(2,1)S(1)}, bf16[96,2048]{1,0:T(8,128)(2,1)}, u32[]{:S(2)}) copy-start(bf16[96,2048]{1,0:T(8,128)(2,1)} %param.27) | copy-start | bytes 1179652
  152.6 898.7 %all-gather.6.cloned.1.call-start = ((), (), s32[]{:S(2)}) async-start(), calls=%async_computation.3 | async-start | bytes 3538944 | tf_op jit(solution)/shard_map/all_gather | solution.py:153
  194.8 909.5 %reduce-scatter.2.cloned.1.call-start = ((), (), s32[]{:S(2)}) async-start(), calls=%async_computation.5 | async-start | bytes 3538944 | tf_op jit(solution)/shard_map/reduce_scatter | solution.py:157
  (7 other events, 15.9 us)
Sparse Core Ops, SparseCore 0:
  11.8 108.4 all-gather.3
  122.4 78.2 all-gather.7
  202.4 848.8 all-gather.5
  1068.4 35.8 reduce-scatter.1
where the time goes:
time: 1120 us; the launch traced here: 1110 us
  waiting for transfers between devices  979 us (87%)
  other arithmetic  49.7 us (4%)
  local copies, waits for them, and re-layouts  37.1 us (3%)
  matrix products  28.7 us (3%)
  between operations  13.8 us (1%)
    all_gather x1, waiting for transfers between devices, on_device(): normed_rows = lax.all_gather(normed, 'tp', axis=0, tiled=True)  851 us
    all_gather x2, waiting for transfers between devices, turned_gather(): whole, at, done = (lax.all_gather(both, axis, axis=0, tiled=True), 0, [])  53.7 us
    all_to_all x1, waiting for transfers between devices, summed_on_arrival(): lax.all_to_all(pieces, axis, split_axis=0, concat_axis=0, tiled=True)  38.3 us
    reduce_scatter x1, waiting for transfers between devices, on_device(): lax.psum_scatter(jnp.dot(hidden, down_full, preferred_element_type=jnp.fl...  36 us
    another operation x4, other arithmetic  23 us
  transfers between devices with their start and end apart: 5, of which 5 were waited for; matrix products, arithmetic and copies ran while one was open for 8% of the time, Pallas kernels for 0%

commit v1 on v0

v1 whole, which is shorter than its diff:
```python
import functools

import jax
import jax.numpy as jnp
import numpy as np
from jax import lax
from jax.experimental import pallas as pl
from jax.experimental.pallas import tpu as pltpu
from jax.sharding import PartitionSpec as P

LOG2E = 1.4426950408889634
CEILING = 30.0
BLOCK = 768
HALF = 384
ROWS = 784
LANES = 256
FOLD = 3
CHUNK = 128
SCALES = (64**-0.5 * LOG2E, 64**-0.5 * LOG2E, 128**-0.5 * LOG2E)


def attention_chunk(q_ref, kv_ref, tri, acc, carry, row, head, shift):
    col = 0 if head < 2 else 256
    rows = pl.ds(row, CHUNK)
    q = q_ref[0, head, rows, :]
    es, ds, values = [], [], []
    for c in range(FOLD):
        keys = kv_ref[0, c * LANES : (c + 1) * LANES, col : col + 128]
        x = lax.dot_general(q, keys, (((1,), (1,)), ((), ())), preferred_element_type=jnp.float32)
        at = BLOCK + 2 * head + c // 2
        offset = kv_ref[0, at : at + 1, (c % 2) * LANES : (c % 2 + 1) * LANES].astype(jnp.float32)
        x = x * SCALES[head] + offset * LOG2E
        e = jnp.exp2(jnp.minimum(x, CEILING))
        if shift is not None:
            t = lax.broadcasted_iota(jnp.int32, (CHUNK, LANES), 0) + (row + shift)
            s = lax.broadcasted_iota(jnp.int32, (CHUNK, LANES), 1) * FOLD + c
            e = jnp.where(s < t, e, 0.0)
        es.append(e)
        ds.append(1.0 + e)
    log_fail = -jnp.log2(ds[0] * ds[1] * ds[2])
    small = log_fail.astype(jnp.bfloat16)
    later = jnp.dot(small, tri, preferred_element_type=jnp.float32)
    before = carry[head, rows, :]
    scale = jnp.exp2(later + log_fail + before[:, :1])
    total = later[:, :1] + small[:, :1].astype(jnp.float32)
    carry[head, rows, :] = before + total
    result = acc[head, rows, :]
    for c in range(FOLD):
        weights = (es[c] * scale).astype(jnp.bfloat16)
        values = kv_ref[0, c * LANES : (c + 1) * LANES, col + 128 : col + 256]
        result = result + jnp.dot(weights, values, preferred_element_type=jnp.float32)
        if c + 1 < FOLD:
            scale = scale * ds[c]
    acc[head, rows, :] = result


def attention_body(table, q_ref, kv_ref, tri_ref, out_ref, acc, carry):
    step = pl.program_id(0)
    first = table[2, step] == 1

    @pl.when(first)
    def _():
        acc[...] = jnp.zeros_like(acc)
        carry[...] = jnp.zeros_like(carry)

    tri = tri_ref[...]

    def sweep(shift):
        def one(i, _):
            row = pl.multiple_of(i * CHUNK, CHUNK)
            for head in range(3):
                attention_chunk(q_ref, kv_ref, tri, acc, carry, row, head, shift)
            return 0

        lax.fori_loop(0, HALF // CHUNK, one, 0)

    @pl.when(first)
    def _():
        sweep(table[3, step])

    @pl.when(jnp.logical_not(first))
    def _():
        sweep(None)

    @pl.when(table[4, step] == 1)
    def _():
        low = lax.broadcasted_iota(jnp.int32, (HALF, 128), 1) < 64
        out_ref[0, :, :128] = jnp.where(low, acc[0], acc[1]).astype(jnp.bfloat16)
        out_ref[0, :, 128:] = acc[2].astype(jnp.bfloat16)


def attention(table, queries, kv, steps):
    tri = jnp.asarray(np.tril(np.ones((LANES, LANES)), -1), jnp.bfloat16)
    return pl.pallas_call(
        attention_body,
        grid_spec=pltpu.PrefetchScalarGridSpec(
            num_scalar_prefetch=1,
            grid=(steps,),
            in_specs=[
                pl.BlockSpec((1, 3, HALF, 128), lambda i, t: (t[0, i], 0, 0, 0)),
                pl.BlockSpec((1, ROWS, 512), lambda i, t: (t[1, i], 0, 0)),
                pl.BlockSpec((LANES, LANES), lambda i, t: (0, 0)),
            ],
            out_specs=pl.BlockSpec((1, HALF, 256), lambda i, t: (t[0, i], 0, 0)),
            scratch_shapes=[
                pltpu.VMEM((3, HALF, 128), jnp.float32),
                pltpu.VMEM((3, HALF, 128), jnp.float32),
            ],
        ),
        out_shape=jax.ShapeDtypeStruct((2, HALF, 256), jnp.bfloat16),
        compiler_params=pltpu.CompilerParams(
            dimension_semantics=("arbitrary",), vmem_limit_bytes=48 * 2**20
        ),
        name="stick_attention",
    )(table, queries, kv, tri)


def step_table(index, blocks):
    steps = jnp.arange(blocks + 1, dtype=jnp.int32)
    high = 2 * blocks - 1 - index
    count = high // 2 + 1
    on_high = steps < count
    half = jnp.where(on_high, high, index)
    key = jnp.where(on_high, high // 2 - steps, index // 2 - (steps - count))
    first = (steps == 0) | (steps == count)
    last = key == 0
    rows = [jnp.where(on_high, 1, 0), key, first, (half % 2) * HALF, last]
    return jnp.stack([r.astype(jnp.int32) for r in rows])


def zigzag_pairs(blocks, back):
    first, second = [], []
    for i in range(blocks):
        for pairs, h in ((first, 2 * i), (second, 2 * i + 1)):
            to = h if h < blocks else 2 * blocks - 1 - h
            pairs.append((to, i) if back else (i, to))
    return first, second


def packed_keys(key_small, value_small, offset_small, key_large, value_large, offset_large):
    rows = jnp.concatenate([key_small, value_small, key_large, value_large], axis=1)
    rows = rows.reshape(LANES, FOLD, 512).transpose(1, 0, 2).reshape(BLOCK, 512)
    offsets = jnp.concatenate([offset_small, offset_large], axis=0)
    offsets = offsets.reshape(3, LANES, FOLD).transpose(0, 2, 1).reshape(3, BLOCK)
    offsets = jnp.pad(offsets, ((0, 0), (0, 1024 - BLOCK))).reshape(6, 512)
    offsets = jnp.pad(offsets, ((0, ROWS - BLOCK - 6), (0, 0)))
    return jnp.concatenate([rows, offsets], axis=0)


def rms_norm(stream, gain):
    scale = lax.rsqrt(jnp.mean(stream * stream, axis=-1, keepdims=True) + 1e-06)
    return (stream * scale * gain.astype(jnp.float32)).astype(jnp.bfloat16)


def on_device(
    query_small,
    key_small,
    value_small,
    offset_small,
    query_large,
    key_large,
    value_large,
    offset_large,
    out_small,
    out_large,
    residual,
    norm_gain,
    gate_weight,
    up_weight,
    down_weight,
):
    blocks = lax.axis_size("sp")
    index = lax.axis_index("sp")
    kv = packed_keys(key_small, value_small, offset_small, key_large, value_large, offset_large)
    kv = lax.all_gather(kv, "sp", axis=0)
    gate_up = lax.all_gather(
        jnp.concatenate([gate_weight, up_weight], axis=1), "sp", axis=0, tiled=True
    )
    down = lax.all_gather(down_weight, "sp", axis=0)

    queries = jnp.concatenate([query_small, query_large], axis=1)
    first, second = zigzag_pairs(blocks, False)
    one = lax.ppermute(queries[:HALF], "sp", first)
    two = lax.ppermute(queries[HALF:], "sp", second)
    even = index % 2 == 0
    low, high = jnp.where(even, one, two), jnp.where(even, two, one)
    both = jnp.stack([low, high])
    lane = lax.broadcasted_iota(jnp.int32, (1, 1, 128), 2) < 64
    zero = jnp.zeros((), jnp.bfloat16)
    heads = jnp.stack(
        [
            jnp.where(lane, both[:, :, :128], zero),
            jnp.where(lane, zero, both[:, :, :128]),
            both[:, :, 128:],
        ],
        axis=1,
    )
    mixed = attention(step_table(index, blocks), heads, kv, blocks + 1)
    back_first, back_second = zigzag_pairs(blocks, True)
    one = jnp.where(even, mixed[0], mixed[1])
    two = jnp.where(even, mixed[1], mixed[0])
    mixed = jnp.concatenate(
        [lax.ppermute(one, "sp", back_first), lax.ppermute(two, "sp", back_second)], axis=0
    )
    part = jnp.dot(
        mixed, jnp.concatenate([out_small, out_large], axis=0), preferred_element_type=jnp.float32
    ).astype(jnp.bfloat16)
    tp = lax.axis_size("tp")
    arrived = lax.all_to_all(
        part.reshape(tp, -1, part.shape[1]), "tp", split_axis=0, concat_axis=0, tiled=True
    )
    attended = arrived.astype(jnp.float32).sum(axis=0).astype(jnp.bfloat16)
    stream = residual.astype(jnp.float32) + attended.astype(jnp.float32)
    normed = rms_norm(stream, norm_gain)
    normed_rows = lax.all_gather(normed, "tp", axis=0, tiled=True)
    width = gate_weight.shape[1]
    gate = jnp.dot(normed_rows, gate_up[:, :width], preferred_element_type=jnp.float32)
    upper = jnp.dot(normed_rows, gate_up[:, width:], preferred_element_type=jnp.float32)
    hidden = (jax.nn.silu(gate) * upper).astype(jnp.bfloat16)
    down_full = jnp.moveaxis(down, 0, 1).reshape(width, -1)
    summed = lax.psum_scatter(
        jnp.dot(hidden, down_full, preferred_element_type=jnp.float32).astype(jnp.bfloat16),
        "tp",
        scatter_dimension=0,
        tiled=True,
    )
    return (stream + summed.astype(jnp.float32)).astype(jnp.bfloat16)


def solution(mesh):
    return jax.shard_map(
        on_device,
        mesh=mesh,
        in_specs=(
            P("sp", "tp"),
            P("sp", "tp"),
            P("sp", "tp"),
            P("tp", "sp"),
            P("sp", "tp"),
            P("sp", "tp"),
            P("sp", "tp"),
            P("tp", "sp"),
            P("tp", None),
            P("tp", None),
            P(("sp", "tp"), None),
            P(),
            P("sp", "tp"),
            P("sp", "tp"),
            P("tp", "sp"),
        ),
        out_specs=P(("sp", "tp"), None),
        check_vma=False,
    )
```

time: 1120 us -> 335 us (0.30)
  waiting for transfers between devices: 979 us -> 194 us
  Pallas kernels: 0 us -> 71.1 us
  other arithmetic: 49.7 us -> 8.95 us
  local copies, waits for them, and re-layouts: 37.1 us -> 5.01 us
  starting transfers between devices: 4.73 us -> 20.9 us
    all_gather x1, waiting for transfers between devices: 851 us -> 23.6 us  [on_device(): normed_rows = lax.all_gather(normed, 'tp', axis=0, tiled=True)]
    pallas_call x0 -> x1, Pallas kernels: none -> 71.1 us  [attention(): pl.pallas_call(attention_body, grid_spec=pltpu.PrefetchScalarGridSpec(num...]
    another operation x5 -> x3, other arithmetic: 27.6 us -> 0.2 us  [the longest x2 0.16 us: on_device(): jnp.stack([jnp.where(lane, both[:, :, :128], zero), jnp.where(lane, zero,...]
    all_gather x2 -> x3, waiting for transfers between devices: 53.7 us -> 79.8 us  [the longest x1 79.8 us: on_device(): kv = lax.all_gather(kv, 'sp', axis=0)]
    ppermute x0 -> x4, starting transfers between devices: none -> 16.3 us  [the longest x1 8.71 us: on_device(): lax.ppermute(two, 'sp', back_second)]
    slice x2 -> x1, local copies, waits for them, and re-layouts: 16.1 us -> 0.03 us  [on_device(): one = lax.ppermute(queries[:HALF], 'sp', first)]
    ppermute x0 -> x4, waiting for transfers between devices: none -> 15.5 us  [the longest x1 8.03 us: on_device(): two = lax.ppermute(queries[HALF:], 'sp', second)]
    convert_element_type x5 -> x3, other arithmetic: 13.5 us -> 1.9 us  [the longest x1 1.89 us: on_device(): return (stream + summed.astype(jnp.float32)).astype(jnp.bfloat16)]
  transfers between devices with their start and end apart: 5 -> 10, of which waited for: 5 -> 6; matrix products, arithmetic and copies ran while one was open for 8% -> 3% of each run, Pallas kernels for 0% -> 21%
where the time goes in v1:
time: 335 us; the launch traced here: 334 us
  waiting for transfers between devices  194 us (58%)
  Pallas kernels  71.1 us (21%)
  starting transfers between devices  20.9 us (6%)
  matrix products  20.9 us (6%)
  between operations  13.5 us (4%)
  other arithmetic  8.95 us (3%)
  local copies, waits for them, and re-layouts  5.01 us (1%)
    all_gather x1, waiting for transfers between devices, on_device(): kv = lax.all_gather(kv, 'sp', axis=0)  79.8 us
    pallas_call x1, Pallas kernels, attention(): pl.pallas_call(attention_body, grid_spec=pltpu.PrefetchScalarGridSpec(num...  71.1 us
    all_to_all x1, waiting for transfers between devices, on_device(): lax.all_to_all(part.reshape(tp, -1, part.shape[1]), 'tp', split_axis=0, c...  38.3 us
    reduce_scatter x1, waiting for transfers between devices, on_device(): lax.psum_scatter(jnp.dot(hidden, down_full, preferred_element_type=jnp.fl...  36 us
    all_gather x1, waiting for transfers between devices, on_device(): normed_rows = lax.all_gather(normed, 'tp', axis=0, tiled=True)  23.6 us
    dot_general x1, matrix products, on_device(): jnp.dot(hidden, down_full, preferred_element_type=jnp.float32)  11.7 us
    ppermute x1, starting transfers between devices, on_device(): lax.ppermute(two, 'sp', back_second)  8.71 us
    ppermute x1, waiting for transfers between devices, on_device(): two = lax.ppermute(queries[HALF:], 'sp', second)  8.03 us
  transfers between devices with their start and end apart: 10, of which 6 were waited for; matrix products, arithmetic and copies ran while one was open for 3% of the time, Pallas kernels for 21%

profile of v1, /device:TPU:0, one launch (start us, length us, event | category | flops | bytes accessed | tf_op | source)
XLA Modules:
  0.0 334.3 jit_solution(8742341374441074509)
XLA Ops:
  6.5 1.3 pad_maximum_fusion
  9.1 1.0 fusion.14
  10.2 0.7 all-gather.13.cloned.1.call-update
  11.0 0.8 pad_maximum_fusion.2
  11.9 0.7 collective-permute-start
  12.6 6.2 %collective-permute-start.1 = (bf16[384,256]{1,0:T(8,128)(2,1)S(1)}, bf16[384,256]{1,0:T(8,128)(2,1)S(1)}, u32[]{:S(2)}, u32[]{:S(2)}) collective-permute-start(bf16[384,256]{1,0:T(8,128)(2,1)S(1)} %get-tuple-element.15), channel_id=1, source_target_pairs={{0,8},{8,24},{16,40},{24,56},{32,72},{40,88},{48,104},{56,120},{64... | collective-permute-start | bytes 589832 | tf_op jit(solution)/shard_map/ppermute | solution.py:184
  18.9 8.0 %collective-permute-done.1 = bf16[384,256]{1,0:T(8,128)(2,1)S(1)} collective-permute-done((bf16[384,256]{1,0:T(8,128)(2,1)S(1)}, bf16[384,256]{1,0:T(8,128)(2,1)S(1)}, u32[]{:S(2)}, u32[]{:S(2)}) %collective-permute-start.1) | collective-permute-done | bytes 196640 | tf_op jit(solution)/shard_map/ppermute | solution.py:184
  27.2 79.8 %all-gather.11.cloned.1.call-done = bf16[12544,512]{1,0:T(8,128)(2,1)} async-done(((bf16[784,512]{1,0:T(8,128)(2,1)}), bf16[12544,512]{1,0:T(8,128)(2,1)}) %all-gather.11.cloned.1.call-update) | async-done | bytes 12845072 | tf_op jit(solution)/shard_map/all_gather | solution.py:175
  107.0 71.1 %stick_attention.1 = bf16[2,384,256]{2,1,0:T(8,128)(2,1)S(1)} custom-call(s32[5,17]{1,0:T(8,128)S(1)} %stack.29.table, bf16[2,3,384,128]{3,2,1,0:T(8,128)(2,1)S(1)} %pad_maximum_fusion.1.q_ref, bf16[16,784,512]{2,1,0:T(8,128)(2,1)} %bitcast.33, bf16[256,256]{1,0:T(8,128)(2,1)S(1)} %copy-done), custom_call_target="tpu_custom_call" | custom-call | tf_op jit(solution)/shard_map/stick_attention/pallas_call | solution.py:94
  178.1 0.7 collective-permute-start.2
  178.8 8.7 %collective-permute-start.3 = (bf16[384,256]{1,0:T(8,128)(2,1)S(1)}, bf16[384,256]{1,0:T(8,128)(2,1)S(1)}, u32[]{:S(2)}, u32[]{:S(2)}) collective-permute-start(bf16[384,256]{1,0:T(8,128)(2,1)S(1)} %get-tuple-element.10), channel_id=1, source_target_pairs={{8,0},{24,8},{40,16},{56,24},{72,32},{88,40},{104,48},{120,56},{11... | collective-permute-start | bytes 589832 | tf_op jit(solution)/shard_map/ppermute | solution.py:203
  187.5 7.4 %collective-permute-done.3 = bf16[384,256]{1,0:T(8,128)(2,1)S(1)} collective-permute-done((bf16[384,256]{1,0:T(8,128)(2,1)S(1)}, bf16[384,256]{1,0:T(8,128)(2,1)S(1)}, u32[]{:S(2)}, u32[]{:S(2)}) %collective-permute-start.3) | collective-permute-done | bytes 196640 | tf_op jit(solution)/shard_map/ppermute | solution.py:203
  195.0 2.6 convolution_convert_fusion.1
  197.6 4.3 %all-to-all-start = ((bf16[8,96,2048]{2,1,0:T(8,128)(2,1)}), bf16[8,96,2048]{2,1,0:T(8,128)(2,1)S(1)}, u32[]{:S(2)}, u32[]{:S(2)}) async-start(bf16[8,96,2048]{2,1,0:T(8,128)(2,1)} %bitcast.13), calls=%async_computation | async-start | bytes 6291456 | tf_op jit(solution)/shard_map/all_to_all | solution.py:209
  201.9 38.3 %all-to-all-done = bf16[8,96,2048]{2,1,0:T(8,128)(2,1)S(1)} async-done(((bf16[8,96,2048]{2,1,0:T(8,128)(2,1)}), bf16[8,96,2048]{2,1,0:T(8,128)(2,1)S(1)}, u32[]{:S(2)}, u32[]{:S(2)}) %all-to-all-start) | async-done | bytes 3145760 | tf_op jit(solution)/shard_map/all_to_all | solution.py:209
  240.3 0.6 reduce_sum.21
  240.9 1.2 multiply_reduce_fusion
  242.1 1.9 multiply_convert_fusion.1
  244.3 3.7 %copy.28 = bf16[16,704,128]{2,0,1:T(8,128)(2,1)S(1)} copy(bf16[16,704,128]{2,1,0:T(8,128)(2,1)} %bitcast.36) | data formatting | bytes 5767168 | tf_op jit(solution)/shard_map/all_gather | solution.py:179
  248.0 23.6 %all-gather.7.cloned.1.call-done = bf16[768,2048]{1,0:T(8,128)(2,1)} async-done(((bf16[96,2048]{1,0:T(8,128)(2,1)}), bf16[768,2048]{1,0:T(8,128)(2,1)}) %all-gather.7.cloned.1.call-update) | async-done | bytes 3145744 | tf_op jit(solution)/shard_map/all_gather | solution.py:215
  271.6 6.6 %fusion.4 = f32[768,704]{0,1:T(8,128)} fusion(bf16[768,2048]{1,0:T(8,128)(2,1)} %all-gather.7.cloned.1.call-done, bf16[2048,1408]{0,1:T(8,128)(2,1)} %all-gather.9.cloned.1.call-done), kind=kOutput, calls=%fused_computation.6 | convolution fusion | flops 2214592512 | bytes 8192000 | tf_op jit(solution)/shard_map/dot_general | solution.py:217
  278.2 11.7 %convolution_convert_fusion = bf16[768,2048]{1,0:T(8,128)(2,1)} fusion(bf16[88,8,16,128]{3,2,1,0:T(8,128)(2,1)S(1)} %bitcast.37, f32[768,704]{0,1:T(8,128)} %fusion.4, bf16[768,2048]{1,0:T(8,128)(2,1)} %all-gather.7.cloned.1.call-done, bf16[2048,1408]{0,1:T(8,128)(2,1)} %all-gather.9.cloned.1.call-done), kind=kOutput, calls=%fused_computation | convolution fusion | flops 4434001920 | bytes 14221312 | tf_op jit(solution)/shard_map/dot_general | solution.py:222
  289.9 36.0 %reduce-scatter.2.cloned.1.call-done = bf16[96,2048]{1,0:T(8,128)(2,1)} async-done(((bf16[768,2048]{1,0:T(8,128)(2,1)}), bf16[96,2048]{1,0:T(8,128)(2,1)}) %reduce-scatter.2.cloned.1.call-update) | async-done | bytes 393232 | tf_op jit(solution)/shard_map/reduce_scatter | solution.py:221
  325.9 1.9 add_convert_fusion
  (57 shorter events, 2.1 us)
Async XLA Ops:
  6.5 2.0 copy-start.10
  6.5 2.0 copy-start.9
  6.5 100.4 %all-gather.11.cloned.1.call-start = ((), (), s32[]{:S(2)}) async-start(), calls=%async_computation.5 | async-start | bytes 13647872 | tf_op jit(solution)/shard_map/all_gather | solution.py:175
  8.3 2.6 copy-start.6
  8.4 2.6 copy-start.7
  8.4 3.4 %copy-start.4 = (bf16[768,128]{1,0:T(8,128)(2,1)S(1)}, bf16[768,128]{1,0:T(8,128)(2,1)}, u32[]{:S(2)}) copy-start(bf16[768,128]{1,0:T(8,128)(2,1)} %param.16) | copy-start | bytes 589828
  8.4 3.4 %copy-start.5 = (bf16[768,128]{1,0:T(8,128)(2,1)S(1)}, bf16[768,128]{1,0:T(8,128)(2,1)}, u32[]{:S(2)}) copy-start(bf16[768,128]{1,0:T(8,128)(2,1)} %param.20) | copy-start | bytes 589828
  10.1 234.2 %all-gather.13.cloned.1.call-start = ((), (), s32[]{:S(2)}) async-start(), calls=%async_computation.6 | async-start | bytes 3063808 | tf_op jit(solution)/shard_map/all_gather | solution.py:179
  10.9 96.1 %copy-start = (bf16[256,256]{1,0:T(8,128)(2,1)S(1)}, bf16[256,256]{1,0:T(8,128)(2,1)}, u32[]{:S(2)}) copy-start(bf16[256,256]{1,0:T(8,128)(2,1)} %constant.72.clone.tri_ref) | copy-start | bytes 393220
  10.9 237.1 %all-gather.9.cloned.1.call-start = ((), (), s32[]{:S(2)}) async-start(), calls=%async_computation.3 | async-start | bytes 6127616 | tf_op jit(solution)/shard_map/all_gather | solution.py:176
  11.9 7.0 %collective-permute-start = (bf16[384,256]{1,0:T(8,128)(2,1)S(1)}, bf16[384,256]{1,0:T(8,128)(2,1)S(1)}, u32[]{:S(2)}, u32[]{:S(2)}) collective-permute-start(bf16[384,256]{1,0:T(8,128)(2,1)S(1)} %get-tuple-element.14), channel_id=1, source_target_pairs={{0,0},{8,16},{16,32},{24,48},{32,64},{40,80},{48,96},{56,112},{64,... | collective-permute-start | bytes 589832 | tf_op jit(solution)/shard_map/ppermute | solution.py:183
  12.6 14.4 %collective-permute-start.1 = (bf16[384,256]{1,0:T(8,128)(2,1)S(1)}, bf16[384,256]{1,0:T(8,128)(2,1)S(1)}, u32[]{:S(2)}, u32[]{:S(2)}) collective-permute-start(bf16[384,256]{1,0:T(8,128)(2,1)S(1)} %get-tuple-element.15), channel_id=1, source_target_pairs={{0,8},{8,24},{16,40},{24,56},{32,72},{40,88},{48,104},{56,120},{64... | collective-permute-start | bytes 589832 | tf_op jit(solution)/shard_map/ppermute | solution.py:184
  107.0 88.0 %copy-start.2 = (bf16[128,2048]{1,0:T(8,128)(2,1)S(1)}, bf16[128,2048]{1,0:T(8,128)(2,1)}, u32[]{:S(2)}) copy-start(bf16[128,2048]{1,0:T(8,128)(2,1)} %param.25) | copy-start | bytes 1572868
  107.0 88.0 %copy-start.3 = (bf16[128,2048]{1,0:T(8,128)(2,1)S(1)}, bf16[128,2048]{1,0:T(8,128)(2,1)}, u32[]{:S(2)}) copy-start(bf16[128,2048]{1,0:T(8,128)(2,1)} %param.24) | copy-start | bytes 1572868
  178.1 9.4 %collective-permute-start.2 = (bf16[384,256]{1,0:T(8,128)(2,1)S(1)}, bf16[384,256]{1,0:T(8,128)(2,1)S(1)}, u32[]{:S(2)}, u32[]{:S(2)}) collective-permute-start(bf16[384,256]{1,0:T(8,128)(2,1)S(1)} %get-tuple-element.9), channel_id=1, source_target_pairs={{0,0},{16,8},{32,16},{48,24},{64,32},{80,40},{96,48},{112,56},{120... | collective-permute-start | bytes 589832 | tf_op jit(solution)/shard_map/ppermute | solution.py:203
  178.8 16.2 %collective-permute-start.3 = (bf16[384,256]{1,0:T(8,128)(2,1)S(1)}, bf16[384,256]{1,0:T(8,128)(2,1)S(1)}, u32[]{:S(2)}, u32[]{:S(2)}) collective-permute-start(bf16[384,256]{1,0:T(8,128)(2,1)S(1)} %get-tuple-element.10), channel_id=1, source_target_pairs={{8,0},{24,8},{40,16},{56,24},{72,32},{88,40},{104,48},{120,56},{11... | collective-permute-start | bytes 589832 | tf_op jit(solution)/shard_map/ppermute | solution.py:203
  197.6 4.3 %copy-start.8 = (bf16[2048]{0:T(1024)(128)(2,1)S(1)}, bf16[2048]{0:T(1024)(128)(2,1)}, u32[]{:S(2)}) copy-start(bf16[2048]{0:T(1024)(128)(2,1)} %param.27) | copy-start | bytes 12292
  197.6 42.7 %all-to-all-start = ((bf16[8,96,2048]{2,1,0:T(8,128)(2,1)}), bf16[8,96,2048]{2,1,0:T(8,128)(2,1)S(1)}, u32[]{:S(2)}, u32[]{:S(2)}) async-start(bf16[8,96,2048]{2,1,0:T(8,128)(2,1)} %bitcast.13), calls=%async_computation | async-start | bytes 6291456 | tf_op jit(solution)/shard_map/all_to_all | solution.py:209
  201.9 69.7 %all-gather.7.cloned.1.call-start = ((), (), s32[]{:S(2)}) async-start(), calls=%async_computation.2 | async-start | bytes 3538944 | tf_op jit(solution)/shard_map/all_gather | solution.py:215
  244.0 81.9 %reduce-scatter.2.cloned.1.call-start = ((), (), s32[]{:S(2)}) async-start(), calls=%async_computation.4 | async-start | bytes 3538944 | tf_op jit(solution)/shard_map/reduce_scatter | solution.py:221
  289.9 36.0 %copy-start.1 = (bf16[96,2048]{1,0:T(8,128)(2,1)S(1)}, bf16[96,2048]{1,0:T(8,128)(2,1)}, u32[]{:S(2)}) copy-start(bf16[96,2048]{1,0:T(8,128)(2,1)} %param.26) | copy-start | bytes 1179652
Sparse Core Ops, SparseCore 0:
  10.3 96.6 all-gather.10
  109.1 46.8 all-gather.12
  158.1 63.9 all-gather.8
  244.2 27.3 all-gather.6
  290.0 35.8 reduce-scatter.1
